TPU v7x, 32 devices: a whole 2x2x4 slice. The times are simulated.
32 devices in a mesh: sp: 16 (over z, y, x), tp: 2 (over core).
Axes of the slice: x: 2, y: 2, z: 4, core: 2. Of those that a mesh axis runs over, the one named last changes fastest.
Arguments:
- latent: bfloat16 [4096, 2048], P(('sp', 'tp')), may hold values from -3 to 3
- context: bfloat16 [1024, 2048], P('sp'), may hold values from -6 to 6
- condition: float32 [2048], replicated, may hold values from -6 to 6
- ctx_cond: float32 [2048], replicated, may hold values from -6 to 6
- norm_gain: float32 [2048], replicated, may hold values from 0.1 to 1.9
- w_shift: bfloat16 [2048, 2048], P('sp', 'tp'), may hold values from -0.25 to 0.25
- w_scale: bfloat16 [2048, 2048], P('sp', 'tp'), may hold values from -0.25 to 0.25
- w_gate: bfloat16 [2048, 2048], P('sp', 'tp'), may hold values from -0.25 to 0.25
- w_query: bfloat16 [2048, 2048], P(None, 'tp'), may hold values from -0.125 to 0.125
- w_key: bfloat16 [2048, 2048], P(None, 'tp'), may hold values from -0.125 to 0.125
- w_value: bfloat16 [2048, 2048], P(None, 'tp'), may hold values from -0.125 to 0.125
- w_out: bfloat16 [2048, 2048], P('tp'), may hold values from -0.125 to 0.125
- rel_bias: float32 [16, 15, 31], replicated, may hold values from 2 to 250
Outputs:
- updated: bfloat16 [4096, 2048], P(('sp', 'tp'))
All inputs are finite; a program needn't handle non-finite values.
Results may differ from a plain program's by a relative error of at most 0.015.
Values may be sent and summed in bfloat16 or wider, within the bound.
A program may use at most 128 MiB of HBM per device.

v0:
```python
import jax
import jax.numpy as jnp
from jax import lax
from jax.sharding import PartitionSpec as P

HEADS = 16
HEAD_DIM = 128
GRID_W = 32
WIN_H = 8
WIN_W = 16
NORM_EPS = 1e-06
NEG_BIG = -1e30


def padded_2(cells, sides, width):
    for axis, dim in sides:
        count = lax.axis_size(axis)
        ends = count - 1
        head = lax.slice_in_dim(cells, 0, width, axis=dim)
        tail = lax.slice_in_dim(cells, cells.shape[dim] - width, cells.shape[dim], axis=dim)
        cells = jnp.concatenate(
            [
                lax.ppermute(tail, axis, [(i, (i + 1) % count) for i in range(ends)]),
                cells,
                lax.ppermute(head, axis, [((i + 1) % count, i) for i in range(ends)]),
            ],
            axis=dim,
        )
    return cells


def rms_mod(block, norm_gain, shifts, scales):
    block = block.astype(jnp.float32)
    normed = (
        block * lax.rsqrt(jnp.mean(block * block, axis=-1, keepdims=True) + NORM_EPS) * norm_gain
    )
    return (normed * (1.0 + scales) + shifts).astype(jnp.bfloat16)


def project(block, weights):
    return jnp.stack(
        [
            jnp.dot(block, weight, preferred_element_type=jnp.float32).astype(jnp.bfloat16)
            for weight in weights
        ]
    )


def on_device(
    latent,
    context,
    condition,
    ctx_cond,
    norm_gain,
    w_shift,
    w_scale,
    w_gate,
    w_query,
    w_key,
    w_value,
    w_out,
    rel_bias,
):
    tp_size = lax.axis_size("tp")
    sp_size = lax.axis_size("sp")
    head_dev = HEADS // tp_size
    head_cols = w_query.shape[1]
    model_width = w_query.shape[0]
    row_part = w_shift.shape[0]
    col_part = w_shift.shape[1]
    activated = jax.nn.silu(jnp.stack([condition, ctx_cond])).astype(jnp.bfloat16)
    act_rows = lax.dynamic_slice_in_dim(activated, lax.axis_index("sp") * row_part, row_part, 1)
    partial_value = jnp.concatenate(
        [
            jnp.dot(act_rows, w_shift, preferred_element_type=jnp.float32),
            jnp.dot(act_rows, w_scale, preferred_element_type=jnp.float32),
            jnp.dot(act_rows[:1], w_gate, preferred_element_type=jnp.float32),
        ],
        axis=0,
    )
    placed = lax.dynamic_update_slice_in_dim(
        jnp.zeros((5, model_width), jnp.float32), partial_value, lax.axis_index("tp") * col_part, 1
    )
    mod_vecs = lax.psum(placed, ("sp", "tp"))
    normed = rms_mod(latent, norm_gain, mod_vecs[0], mod_vecs[2])
    projected = project(lax.all_gather(normed, "tp", axis=0, tiled=True), (w_query, w_key, w_value))
    ctx_kv = lax.all_gather(
        project(rms_mod(context, norm_gain, mod_vecs[1], mod_vecs[3]), (w_key, w_value)),
        "sp",
        axis=1,
        tiled=True,
    )
    ctx_key3 = ctx_kv[0].reshape(-1, head_dev, HEAD_DIM)
    ctx_val3 = ctx_kv[1].reshape(-1, head_dev, HEAD_DIM)
    grid_rows = projected.shape[1] // GRID_W
    queries = projected[0].reshape(grid_rows, GRID_W, head_dev, HEAD_DIM)
    half_win = WIN_H // 2
    padded = padded_2(
        projected[1:].reshape(2, grid_rows, GRID_W, head_cols), (("sp", 1),), half_win
    )
    total_rows = grid_rows * sp_size
    first_row = lax.axis_index("sp") * grid_rows
    local_rows = jnp.arange(grid_rows, dtype=jnp.int32)
    starts = (
        jnp.clip(first_row + local_rows - half_win, 0, total_rows - WIN_H) - first_row + half_win
    )

    def take_window(start_row):
        return lax.dynamic_slice_in_dim(padded, start_row, WIN_H, 1)

    windows = jax.vmap(take_window)(starts)
    key_win = windows[:, 0].reshape(grid_rows, WIN_H, GRID_W, head_dev, HEAD_DIM)
    val_win = windows[:, 1].reshape(grid_rows, WIN_H, GRID_W, head_dev, HEAD_DIM)
    row_off = (
        starts[:, None]
        - half_win
        + jnp.arange(WIN_H, dtype=jnp.int32)[None, :]
        - local_rows[:, None]
        + WIN_H
        - 1
    )
    col_ids = jnp.arange(GRID_W, dtype=jnp.int32)
    col_start = jnp.clip(col_ids - WIN_W // 2, 0, GRID_W - WIN_W)
    col_in = (col_ids[None, :] >= col_start[:, None]) & (
        col_ids[None, :] < col_start[:, None] + WIN_W
    )
    col_off = jnp.clip(col_ids[None, :] - col_ids[:, None], 1 - WIN_W, WIN_W - 1) + WIN_W - 1
    col_hot = (col_off[:, :, None] == jnp.arange(2 * WIN_W - 1)[None, None, :]).astype(jnp.float32)
    row_hot = (row_off[:, :, None] == jnp.arange(2 * WIN_H - 1)[None, None, :]).astype(jnp.float32)
    bias_table = lax.dynamic_slice_in_dim(rel_bias, lax.axis_index("tp") * head_dev, head_dev, 0)
    col_table = jnp.einsum("hec,qwc->heqw", bias_table, col_hot, precision=lax.Precision.HIGHEST)
    bias_win = jnp.einsum("rke,heqw->rqhkw", row_hot, col_table, precision=lax.Precision.HIGHEST)
    inv_scale = HEAD_DIM ** (-0.5)
    scores_win = (
        jnp.einsum("rqhd,rkwhd->rqhkw", queries, key_win, preferred_element_type=jnp.float32)
        * inv_scale
        + bias_win
    )
    scores_win = jnp.where(col_in[None, :, None, None, :], scores_win, NEG_BIG)
    scores_win = scores_win.reshape(grid_rows, GRID_W, head_dev, WIN_H * GRID_W)
    scores_ctx = (
        jnp.einsum("rqhd,chd->rqhc", queries, ctx_key3, preferred_element_type=jnp.float32)
        * inv_scale
    )
    row_max = jnp.maximum(jnp.max(scores_win, axis=-1), jnp.max(scores_ctx, axis=-1))
    exp_win = jnp.exp(scores_win - row_max[..., None])
    exp_ctx = jnp.exp(scores_ctx - row_max[..., None])
    row_total = jnp.sum(exp_win, axis=-1) + jnp.sum(exp_ctx, axis=-1)
    probs_win = (exp_win / row_total[..., None]).astype(jnp.bfloat16)
    probs_win = probs_win.reshape(grid_rows, GRID_W, head_dev, WIN_H, GRID_W)
    probs_ctx = (exp_ctx / row_total[..., None]).astype(jnp.bfloat16)
    attended = jnp.einsum(
        "rqhkw,rkwhd->rqhd", probs_win, val_win, preferred_element_type=jnp.float32
    )
    attended = attended + jnp.einsum(
        "rqhc,chd->rqhd", probs_ctx, ctx_val3, preferred_element_type=jnp.float32
    )
    attended = attended.astype(jnp.bfloat16).reshape(grid_rows * GRID_W, head_cols)
    branch = lax.psum_scatter(
        jnp.dot(attended, w_out, preferred_element_type=jnp.float32).astype(jnp.bfloat16),
        "tp",
        scatter_dimension=0,
        tiled=True,
    ).astype(jnp.float32)
    return (latent.astype(jnp.float32) + mod_vecs[4] * branch).astype(jnp.bfloat16)


def solution(mesh):
    placed = (
        P(("sp", "tp"), None),
        P("sp", None),
        P(),
        P(),
        P(),
        P("sp", "tp"),
        P("sp", "tp"),
        P("sp", "tp"),
        P(None, "tp"),
        P(None, "tp"),
        P(None, "tp"),
        P("tp", None),
        P(),
    )
    return jax.shard_map(
        on_device, mesh=mesh, in_specs=placed, out_specs=P(("sp", "tp"), None), check_vma=False
    )
```

profile of v0, /device:TPU:0, one launch (start us, length us, event | category | flops | bytes accessed | tf_op | source)
XLA Modules:
  0.0 193.7 jit_solution(12751256618278326930)
XLA Ops:
  6.6 0.8 fusion.61
  7.4 0.2 copy-done
  7.5 0.1 fusion.69
  7.7 1.1 fusion.70
  8.8 1.1 fusion.63
  9.9 42.3 %psum.7 = f32[5,2048]{1,0:T(8,128)S(1)} all-reduce(f32[5,2048]{1,0:T(8,128)S(1)} %maximum_dynamic-update-slice_fusion), channel_id=1, replica_groups=mesh['sp'=16,'tp'=2] {'sp','tp'}, use_global_device_ids=true, to_apply=%region_0.1 | all-reduce | flops 10240 | bytes 81920 | tf_op jit(solution)/shard_map/psum | solution.py:84
  52.2 1.2 fusion.35
  53.5 2.1 %fusion.39 = bf16[128,2048]{1,0:T(8,128)(2,1)} fusion(bf16[128,2048]{1,0:T(8,128)(2,1)} %param.13, f32[2048]{0:T(1024)S(1)} %bitcast.155, f32[2048]{0:T(1024)S(1)} %bitcast.156, f32[2048]{0:T(1024)} %param.17, f32[128]{0:T(128)S(1)} %add_rsqrt_fusion.1), kind=kLoop, calls=%fused_computation.46 | loop fusion | flops 1572864 | bytes 1073664 | tf_op jit(solution)/shard_map/convert_element_type | solution.py:37
  55.6 0.0 all-gather.3.cloned.1.call-update
  55.6 0.0 all-gather.5.cloned.1.call-start
  55.7 0.0 copy-start.3
  55.7 1.3 fusion.41
  56.9 0.0 copy-start.8
  57.0 3.2 %fusion.33 = bf16[1,64,1024]{2,1,0:T(8,128)(2,1)S(1)} fusion(bf16[2048,1024]{1,0:T(8,128)(2,1)} %param.22, bf16[64,2048]{1,0:T(8,128)(2,1)} %param.14, f32[2048]{0:T(1024)S(1)} %bitcast.150, f32[2048]{0:T(1024)S(1)} %bitcast.152, f32[2048]{0:T(1024)} %param.17, f32[64]{0:T(128)S(1)} %add_rsqrt_fusion), kind=kOutput, calls=%fused_computation.40 | convolution fusion | flops 269287424 | bytes 4612352 | tf_op jit(solution)/shard_map/dot_general | solution.py:43
  60.2 0.9 fusion.34
  61.1 0.7 pad_maximum_fusion.2
  61.9 0.0 all-gather.5.cloned.1.call-update
  61.9 0.0 reduce-scatter.2.cloned.1.call-start
  62.0 0.1 subtract_add_fusion
  62.1 1.4 fusion.51
  63.5 5.6 %fusion.12 = f32[8,32,32,8,8]{2,4,3,1,0:T(8,128)} fusion(f32[8,15,32,32]{3,1,2,0:T(8,128)S(1)} %fusion.51, s32[8,8]{1,0:T(8,128)S(1)} %subtract_add_fusion), kind=kOutput, calls=%fused_computation.21 | convolution fusion | flops 94372800 | bytes 2588928 | tf_op jit(solution)/shard_map/rke,heqw->rqhkw/dot_general | solution.py:132
  69.2 9.3 %copy.59 = f32[8,32,32,8,8]{1,2,4,0,3:T(8,128)} copy(f32[8,32,32,8,8]{2,4,3,1,0:T(8,128)} %fusion.12) | data formatting | bytes 4194304 | tf_op jit(solution)/shard_map/rke,heqw->rqhkw/dot_general | solution.py:132
  78.5 0.0 all-gather.3.cloned.1.call-done
  78.5 0.0 copy-start.4
  78.5 3.9 %convolution_convert_fusion.2 = bf16[256,1024]{1,0:T(8,128)(2,1)S(1)} fusion(bf16[256,2048]{1,0:T(8,128)(2,1)} %all-gather.3.cloned.1.call-done, bf16[2048,1024]{1,0:T(8,128)(2,1)} %param.23), kind=kOutput, calls=%fused_computation.35 | convolution fusion | flops 1074003968 | bytes 5767168 | tf_op jit(solution)/shard_map/dot_general | solution.py:43
  82.4 0.1 copy-done.10
  82.6 1.3 convolution_convert_fusion.3
  83.8 0.1 fusion.46
  83.9 4.2 %collective-permute-start = (bf16[2,4,32,1024]{3,2,0,1:T(8,128)(2,1)S(1)}, bf16[2,4,32,1024]{3,2,0,1:T(8,128)(2,1)S(1)}, u32[]{:S(2)}, u32[]{:S(2)}) collective-permute-start(bf16[2,4,32,1024]{3,2,0,1:T(8,128)(2,1)S(1)} %get-tuple-element.9), channel_id=1, source_target_pairs={{0,2},{2,4},{4,6},{6,8},{8,10},{10,12},{12,14},{14,16},{16,18},{18... | collective-permute-start | bytes 1572872 | tf_op jit(solution)/shard_map/ppermute | solution.py:23
  88.2 1.3 collective-permute-start.1
  89.5 1.3 fusion.32
  90.8 0.1 copy.82
  90.9 0.1 copy.61
  91.0 25.2 %collective-permute-done = bf16[2,4,32,1024]{3,2,0,1:T(8,128)(2,1)S(1)} collective-permute-done((bf16[2,4,32,1024]{3,2,0,1:T(8,128)(2,1)S(1)}, bf16[2,4,32,1024]{3,2,0,1:T(8,128)(2,1)S(1)}, u32[]{:S(2)}, u32[]{:S(2)}) %collective-permute-start) | collective-permute-done | bytes 524320 | tf_op jit(solution)/shard_map/ppermute | solution.py:23
  116.2 1.9 collective-permute-done.1
  118.1 0.3 pad_maximum_fusion
  118.4 4.9 %gather_fusion = bf16[8,2,8,32,1024]{4,3,1,2,0:T(8,128)(2,1)} fusion(bf16[2,16,32,1024]{3,2,0,1:T(8,128)(2,1)S(1)} %pad_maximum_fusion, s32[8]{0:T(128)S(1)} %shift-left_bitcast_fusion), kind=kCustom, calls=%fused_computation | custom fusion | bytes 16777344 | tf_op jit(solution)/shard_map/vmap()/gather | solution.py:109
  123.3 4.0 %fusion.66 = (bf16[8,1,8,32,1024]{4,3,1,2,0:T(8,128)(2,1)S(1)}, bf16[8,1,8,32,1024]{4,3,1,2,0:T(8,128)(2,1)S(1)}) fusion(bf16[8,2,8,32,1024]{4,3,1,2,0:T(8,128)(2,1)} %gather_fusion), kind=kLoop, calls=%fused_computation.99 | loop fusion | bytes 16777216 | tf_op jit(solution)/shard_map/slice | solution.py:113
  127.3 0.0 slice-start
  127.3 1.1 copy.81
  128.4 0.0 slice-start.1
  128.4 3.3 %copy.80 = bf16[256,8,8,128]{3,2,1,0:T(8,128)(2,1)} copy(bf16[256,8,8,128]{3,1,2,0:T(8,128)(2,1)S(1)} %bitcast.137) | data formatting | bytes 8388608
  131.7 1.2 slice-done.1
  132.9 4.3 %fusion.68 = (f32[8,32,8]{1,2,0:T(8,128)S(1)}, f32[8,32,8,8,32]{1,4,3,2,0:T(8,128)}) fusion(f32[8,32,32,8,8]{1,2,4,0,3:T(8,128)S(1)} %bitcast.133, bf16[8,32,8,128,1]{3,2,1,0,4:T(8,128)(2,1)S(1)} %bitcast_bitcast_fusion, bf16[8,8,32,8,128]{4,3,2,1,0:T(8,128)(2,1)S(1)} %bitcast.136, pred[32,32]{0,1:T(8,128)(4,1)S(1)} %fusion.57), kind=kOutput, calls=%fused_computation.101 | convolution fusion | flops 136312832 | bytes 8922112 | tf_op jit(solution)/shard_map/rqhd,rkwhd->rqhkw/dot_general | solution.py:135
  137.2 19.0 %all-gather.5.cloned.1.call-done = bf16[2,1024,1024]{2,1,0:T(8,128)(2,1)} async-done(((bf16[2,64,1024]{2,1,0:T(8,128)(2,1)}), bf16[2,1024,1024]{2,1,0:T(8,128)(2,1)}) %all-gather.5.cloned.1.call-update) | async-done | bytes 4194320 | tf_op jit(solution)/shard_map/all_gather | solution.py:87
  156.2 3.2 %slice_bitcast_fusion = (bf16[128,8,8,128]{3,1,2,0:T(8,128)(2,1)S(1)}, bf16[128,8,8,128]{3,1,2,0:T(8,128)(2,1)S(1)}) fusion(bf16[2,1024,1024]{2,1,0:T(8,128)(2,1)} %all-gather.5.cloned.1.call-done), kind=kLoop, calls=%fused_computation.18 | loop fusion | bytes 8388608
  159.4 0.6 copy.83
  160.0 1.3 fusion.16
  161.3 0.0 slice-start.2
  161.3 0.7 bitcast_reduce_fusion
  162.0 0.0 slice-start.3
  162.0 1.9 fusion.3
  163.9 1.0 slice-done.3
  164.9 2.0 %fusion.2 = f32[8,32,8]{1,2,0:T(8,128)S(1)} fusion(f32[8,32,8,8,32]{1,4,3,2,0:T(8,128)S(1)} %bitcast.135, f32[8,32,8]{1,2,0:T(8,128)S(1)} %copy_maximum_fusion), kind=kLoop, calls=%fused_computation.9 | loop fusion | flops 1046528 | bytes 2113536 | tf_op jit(solution)/shard_map/reduce_sum | solution.py:148
  167.0 0.6 copy.84
  167.6 3.3 %fusion.21 = f32[8,32,8,128]{3,1,2,0:T(8,128)S(1)} fusion(bf16[1024,8,128]{2,1,0:T(8,128)(2,1)S(1)} %bitcast.143, f32[8,32,8]{1,0,2:T(8,128)S(1)} %copy.67, f32[8,32,8]{1,0,2:T(8,128)S(1)} %copy.63, f32[8,1024,256]{1,2,0:S(1)} %fusion.16), kind=kOutput, calls=%fused_computation.31 | convolution fusion | flops 545259520 | bytes 11550720 | tf_op jit(solution)/shard_map/rqhc,chd->rqhd/dot_general | solution.py:155
  170.9 2.3 %fusion.29 = bf16[8,32,8,128]{3,1,2,0:T(8,128)(2,1)S(1)} fusion(f32[8,32,8,128]{3,1,2,0:T(8,128)S(1)} %fusion.21, f32[8,32,8,8,32]{1,4,3,2,0:T(8,128)S(1)} %bitcast.135, f32[8,32,8]{1,2,0:T(8,128)S(1)} %copy_add_fusion, f32[8,32,8]{1,2,0:T(8,128)S(1)} %copy_maximum_fusion, bf16[8,8,32,8,128]{4,3,2,1,0:T(8,128)(2,1)S(1)} %bitcast.142), kind=kOutput, calls=%fused_computation.33 | convolution fusion | flops 136314880 | bytes 7880704 | tf_op jit(solution)/shard_map/rqhkw,rkwhd->rqhd/dot_general | solution.py:152
  173.2 0.2 copy.70
  173.5 0.0 copy-start.2
  173.5 0.0 copy-start.1
  173.5 4.5 %convolution_convert_fusion = bf16[256,2048]{1,0:T(8,128)(2,1)} fusion(bf16[1024,2048]{1,0:T(8,128)(2,1)} %param.24, bf16[32,8,8,128]{3,2,1,0:T(8,128)(2,1)S(1)} %bitcast.149), kind=kOutput, calls=%fused_computation.17 | convolution fusion | flops 1074266112 | bytes 5767168 | tf_op jit(solution)/shard_map/dot_general | solution.py:160
  178.0 0.0 reduce-scatter.2.cloned.1.call-update
  178.0 7.1 %reduce-scatter.2.cloned.1.call-done = bf16[128,2048]{1,0:T(8,128)(2,1)} async-done(((bf16[256,2048]{1,0:T(8,128)(2,1)}), bf16[128,2048]{1,0:T(8,128)(2,1)}) %reduce-scatter.2.cloned.1.call-update) | async-done | bytes 524304 | tf_op jit(solution)/shard_map/reduce_scatter | solution.py:159
  185.1 2.0 %fusion.40 = bf16[128,2048]{1,0:T(8,128)(2,1)} fusion(bf16[128,2048]{1,0:T(8,128)(2,1)S(1)} %copy-done.2, bf16[128,2048]{1,0:T(8,128)(2,1)} %reduce-scatter.2.cloned.1.call-done, f32[2048]{0:T(1024)S(1)} %bitcast.154), kind=kLoop, calls=%fused_computation.47 | loop fusion | flops 1310720 | bytes 1581056 | tf_op jit(solution)/shard_map/convert_element_type | solution.py:165
  (36 shorter events, 0.2 us)
Async XLA Ops:
  6.5 1.0 copy-start
  6.5 53.7 %copy-start.7 = (f32[2048]{0:T(1024)S(1)}, f32[2048]{0:T(1024)}, u32[]{:S(2)}) copy-start(f32[2048]{0:T(1024)} %param.17) | copy-start | bytes 24580
  6.5 53.7 %copy-start.6 = (bf16[64,2048]{1,0:T(8,128)(2,1)S(1)}, bf16[64,2048]{1,0:T(8,128)(2,1)}, u32[]{:S(2)}) copy-start(bf16[64,2048]{1,0:T(8,128)(2,1)} %param.14) | copy-start | bytes 786436
  6.5 72.0 %all-gather.3.cloned.1.call-start = ((), (), s32[]{:S(2)}) async-start(), calls=%async_computation.1 | async-start | bytes 1572864 | tf_op jit(solution)/shard_map/all_gather | solution.py:86
  55.6 100.6 %all-gather.5.cloned.1.call-start = ((), (), s32[]{:S(2)}) async-start(), calls=%async_computation.2 | async-start | bytes 4456448 | tf_op jit(solution)/shard_map/all_gather | solution.py:87
  55.7 4.6 %copy-start.3 = (bf16[2048,1024]{1,0:T(8,128)(2,1)S(1)}, bf16[2048,1024]{1,0:T(8,128)(2,1)}, u32[]{:S(2)}) copy-start(bf16[2048,1024]{1,0:T(8,128)(2,1)} %param.23) | copy-start | bytes 12582916
  56.9 5.0 %copy-start.8 = (f32[16,15,31]{2,0,1:T(8,128)S(1)}, f32[16,15,31]{2,0,1:T(8,128)}, u32[]{:S(2)}) copy-start(f32[16,15,31]{2,0,1:T(8,128)} %param.25) | copy-start | bytes 89284
  61.9 123.2 %reduce-scatter.2.cloned.1.call-start = ((), (), s32[]{:S(2)}) async-start(), calls=%async_computation.3 | async-start | bytes 1572864 | tf_op jit(solution)/shard_map/reduce_scatter | solution.py:159
  78.5 3.9 %copy-start.4 = (bf16[2048,1024]{1,0:T(8,128)(2,1)S(1)}, bf16[2048,1024]{1,0:T(8,128)(2,1)}, u32[]{:S(2)}) copy-start(bf16[2048,1024]{1,0:T(8,128)(2,1)} %param.22) | copy-start | bytes 12582916
  78.5 4.0 %copy-start.10 = (bf16[256,2048]{1,0:T(8,128)(2,1)S(1)}, bf16[256,2048]{1,0:T(8,128)(2,1)}, u32[]{:S(2)}) copy-start(bf16[256,2048]{1,0:T(8,128)(2,1)} %all-gather.3.cloned.1.call-done) | copy-start | bytes 3145732
  82.6 6.9 %copy-start.9 = (bf16[2048,1024]{1,0:T(8,128)(2,1)S(1)}, bf16[2048,1024]{1,0:T(8,128)(2,1)}, u32[]{:S(2)}) copy-start(bf16[2048,1024]{1,0:T(8,128)(2,1)} %param.21) | copy-start | bytes 12582916
  83.9 32.3 %collective-permute-start = (bf16[2,4,32,1024]{3,2,0,1:T(8,128)(2,1)S(1)}, bf16[2,4,32,1024]{3,2,0,1:T(8,128)(2,1)S(1)}, u32[]{:S(2)}, u32[]{:S(2)}) collective-permute-start(bf16[2,4,32,1024]{3,2,0,1:T(8,128)(2,1)S(1)} %get-tuple-element.9), channel_id=1, source_target_pairs={{0,2},{2,4},{4,6},{6,8},{8,10},{10,12},{12,14},{14,16},{16,18},{18... | collective-permute-start | bytes 1572872 | tf_op jit(solution)/shard_map/ppermute | solution.py:23
  88.2 30.0 %collective-permute-start.1 = (bf16[2,4,32,1024]{3,2,0,1:T(8,128)(2,1)S(1)}, bf16[2,4,32,1024]{3,2,0,1:T(8,128)(2,1)S(1)}, u32[]{:S(2)}, u32[]{:S(2)}) collective-permute-start(bf16[2,4,32,1024]{3,2,0,1:T(8,128)(2,1)S(1)} %get-tuple-element.10), channel_id=1, source_target_pairs={{2,0},{4,2},{6,4},{8,6},{10,8},{12,10},{14,12},{16,14},{18,16},{20... | collective-permute-start | bytes 1572872 | tf_op jit(solution)/shard_map/ppermute | solution.py:25
  127.3 4.5 %slice-start = ((s8[8388608]{0:T(1024)(128)(4,1)}), s8[4194304]{0:T(1024)(128)(4,1)S(1)}, s32[]{:S(2)}) async-start(s8[8388608]{0:T(1024)(128)(4,1)} %bitcast.132), calls=%async_computation.4 | async-start | bytes 8388608
  128.4 4.5 %slice-start.1 = ((s8[8388608]{0:T(1024)(128)(4,1)}), s8[4194304]{0:T(1024)(128)(4,1)S(1)}, s32[]{:S(2)}) async-start(s8[8388608]{0:T(1024)(128)(4,1)} %bitcast.132), calls=%async_computation.5 | async-start | bytes 8388608
  161.3 2.6 %slice-start.2 = ((s8[8388608]{0:T(1024)(128)(4,1)}), s8[4194304]{0:T(1024)(128)(4,1)S(1)}, s32[]{:S(2)}) async-start(s8[8388608]{0:T(1024)(128)(4,1)} %bitcast.134), calls=%async_computation.6 | async-start | bytes 8388608
  162.0 2.9 %slice-start.3 = ((s8[8388608]{0:T(1024)(128)(4,1)}), s8[4194304]{0:T(1024)(128)(4,1)S(1)}, s32[]{:S(2)}) async-start(s8[8388608]{0:T(1024)(128)(4,1)} %bitcast.134), calls=%async_computation.7 | async-start | bytes 8388608
  167.6 3.3 %copy-start.5 = (bf16[256,8,8,128]{3,2,1,0:T(8,128)(2,1)S(1)}, bf16[256,8,8,128]{3,2,1,0:T(8,128)(2,1)}, u32[]{:S(2)}) copy-start(bf16[256,8,8,128]{3,2,1,0:T(8,128)(2,1)} %copy.80) | copy-start | bytes 12582916
  173.5 11.7 %copy-start.2 = (bf16[128,2048]{1,0:T(8,128)(2,1)S(1)}, bf16[128,2048]{1,0:T(8,128)(2,1)}, u32[]{:S(2)}) copy-start(bf16[128,2048]{1,0:T(8,128)(2,1)} %param.13) | copy-start | bytes 1572868
  173.5 13.6 %copy-start.1 = (bf16[128,1024]{1,0:T(8,128)(2,1)S(1)}, bf16[128,1024]{1,0:T(8,128)(2,1)}, u32[]{:S(2)}) copy-start(bf16[128,1024]{1,0:T(8,128)(2,1)} %param.18) | copy-start | bytes 786436
Sparse Core Ops, SparseCore 0:
  55.7 8.8 all-gather.2
  67.3 88.8 all-gather.4
  178.1 6.9 reduce-scatter.1
where the time goes:
time: 194 us
  waiting for transfers between devices  53.3 us (27%)
  blocking collectives  42.3 us (22%)
  matrix products  35.6 us (18%)
  local copies, waits for them, and re-layouts  30 us (15%)
  between operations  13.6 us (7%)
  other arithmetic  13.3 us (7%)
  starting transfers between devices  5.61 us (3%)
    psum x1, blocking collectives, on_device(): mod_vecs = lax.psum(placed, ('sp', 'tp'))  42.3 us
    ppermute x1, waiting for transfers between devices, padded_2(): lax.ppermute(tail, axis, [(i, (i + 1) % count) for i in range(ends)])  25.2 us
    all_gather x1, waiting for transfers between devices, on_device(): lax.all_gather(project(rms_mod(context, norm_gain, mod_vecs[1], mod_vecs[...  19 us
    unnamed x36, local copies, waits for them, and re-layouts  11.5 us
    dot_general x5, matrix products, project(): jnp.dot(block, weight, preferred_element_type=jnp.float32)  10.6 us
    dot_general x1, local copies, waits for them, and re-layouts, on_device(): jnp.einsum('rke,heqw->rqhkw', row_hot, col_table, precision=lax.Precision...  9.27 us
    reduce_scatter x1, waiting for transfers between devices, on_device(): lax.psum_scatter(jnp.dot(attended, w_out, preferred_element_type=jnp.floa...  7.12 us
    dot_general x1, matrix products, on_device(): jnp.einsum('rke,heqw->rqhkw', row_hot, col_table, precision=lax.Precision...  5.61 us
  transfers between devices with their start and end apart: 5, of which 4 were waited for; matrix products, arithmetic and copies ran while one was open for 24% of the time, Pallas kernels for 0%

commit v1 on v0

--- a/solution.py
+++ b/solution.py
@@ -81,7 +81,7 @@
     placed = lax.dynamic_update_slice_in_dim(
         jnp.zeros((5, model_width), jnp.float32), partial_value, lax.axis_index("tp") * col_part, 1
     )
-    mod_vecs = lax.psum(placed, ("sp", "tp"))
+    mod_vecs = lax.psum(lax.psum(placed, "tp"), "sp")
     normed = rms_mod(latent, norm_gain, mod_vecs[0], mod_vecs[2])
     projected = project(lax.all_gather(normed, "tp", axis=0, tiled=True), (w_query, w_key, w_value))
     ctx_kv = lax.all_gather(

time: 194 us -> 222 us (1.14)
  blocking collectives: 42.3 us -> 82.3 us
  waiting for transfers between devices: 53.3 us -> 43.5 us
  starting transfers between devices: 5.61 us -> 2.7 us
    psum x1 -> x2, blocking collectives: 42.3 us -> 82.3 us  [on_device(): mod_vecs = lax.psum(lax.psum(placed, 'tp'), 'sp')]
    ppermute x1, waiting for transfers between devices: 25.2 us -> 16.8 us  [padded_2(): lax.ppermute(tail, axis, [(i, (i + 1) % count) for i in range(ends)])]
    ppermute x1, starting transfers between devices: 4.23 us -> 1.32 us  [padded_2(): lax.ppermute(tail, axis, [(i, (i + 1) % count) for i in range(ends)])]
  transfers between devices with their start and end apart: 5 -> 5, of which waited for: 4 -> 3; matrix products, arithmetic and copies ran while one was open for 24% -> 22% of each run, Pallas kernels for 0% -> 0%
where the time goes in v1:
time: 222 us; the launch traced here: 221 us
  blocking collectives  82.3 us (37%)
  waiting for transfers between devices  43.5 us (20%)
  matrix products  36.1 us (16%)
  local copies, waits for them, and re-layouts  30 us (14%)
  between operations  13.6 us (6%)
  other arithmetic  13.3 us (6%)
  starting transfers between devices  2.7 us (1%)
    psum x2, blocking collectives, on_device(): mod_vecs = lax.psum(lax.psum(placed, 'tp'), 'sp')  82.3 us
    all_gather x1, waiting for transfers between devices, on_device(): lax.all_gather(project(rms_mod(context, norm_gain, mod_vecs[1], mod_vecs[...  19.5 us
    ppermute x1, waiting for transfers between devices, padded_2(): lax.ppermute(tail, axis, [(i, (i + 1) % count) for i in range(ends)])  16.8 us
    unnamed x36, local copies, waits for them, and re-layouts  11.5 us
    dot_general x5, matrix products, project(): jnp.dot(block, weight, preferred_element_type=jnp.float32)  11 us
    dot_general x1, local copies, waits for them, and re-layouts, on_device(): jnp.einsum('rke,heqw->rqhkw', row_hot, col_table, precision=lax.Precision...  9.26 us
    reduce_scatter x1, waiting for transfers between devices, on_device(): lax.psum_scatter(jnp.dot(attended, w_out, preferred_element_type=jnp.floa...  7.12 us
    dot_general x1, matrix products, on_device(): jnp.einsum('rke,heqw->rqhkw', row_hot, col_table, precision=lax.Precision...  5.63 us
  transfers between devices with their start and end apart: 5, of which 3 were waited for; matrix products, arithmetic and copies ran while one was open for 22% of the time, Pallas kernels for 0%

profile of v1, /device:TPU:0, one launch (start us, length us, event | category | flops | bytes accessed | tf_op | source)
XLA Modules:
  0.0 221.4 jit_solution(14409335116672816486)
XLA Ops:
  6.6 0.8 fusion.61
  7.4 0.2 copy-done
  7.5 0.1 fusion.69
  7.7 1.1 fusion.70
  8.8 1.1 fusion.63
  9.9 3.9 %psum.14 = f32[5,2048]{1,0:T(8,128)S(1)} all-reduce(f32[5,2048]{1,0:T(8,128)S(1)} %maximum_dynamic-update-slice_fusion), channel_id=1, replica_groups=mesh['sp'=16,'tp'=2] {'tp'}, use_global_device_ids=true, to_apply=%region_0.1 | all-reduce | flops 10240 | bytes 81920 | tf_op jit(solution)/shard_map/psum | solution.py:84
  13.8 78.3 %psum.15 = f32[5,2048]{1,0:T(8,128)S(1)} all-reduce(f32[5,2048]{1,0:T(8,128)S(1)} %psum.14), channel_id=1, replica_groups=mesh['sp'=16,'tp'=2] {'sp'}, use_global_device_ids=true, to_apply=%region_1.2 | all-reduce | flops 10240 | bytes 81920 | tf_op jit(solution)/shard_map/psum | solution.py:84
  92.2 1.2 fusion.35
  93.4 2.1 fusion.39
  95.5 0.0 all-gather.3.cloned.1.call-update
  95.6 0.0 all-gather.5.cloned.1.call-start
  95.6 0.0 copy-start.3
  95.6 1.3 fusion.41
  96.9 0.0 copy-start.8
  96.9 3.6 %fusion.33 = bf16[1,64,1024]{2,1,0:T(8,128)(2,1)S(1)} fusion(bf16[2048,1024]{1,0:T(8,128)(2,1)} %param.22, bf16[64,2048]{1,0:T(8,128)(2,1)} %param.14, f32[2048]{0:T(1024)S(1)} %bitcast.150, f32[2048]{0:T(1024)S(1)} %bitcast.152, f32[2048]{0:T(1024)} %param.17, f32[64]{0:T(128)S(1)} %add_rsqrt_fusion), kind=kOutput, calls=%fused_computation.40 | convolution fusion | flops 269287424 | bytes 4612352 | tf_op jit(solution)/shard_map/dot_general | solution.py:43
  100.6 0.9 fusion.34
  101.5 0.7 pad_maximum_fusion.2
  102.2 0.0 all-gather.5.cloned.1.call-update
  102.2 0.0 reduce-scatter.2.cloned.1.call-start
  102.4 0.1 subtract_add_fusion
  102.4 1.4 fusion.51
  103.9 5.6 %fusion.12 = f32[8,32,32,8,8]{2,4,3,1,0:T(8,128)} fusion(f32[8,15,32,32]{3,1,2,0:T(8,128)S(1)} %fusion.51, s32[8,8]{1,0:T(8,128)S(1)} %subtract_add_fusion), kind=kOutput, calls=%fused_computation.21 | convolution fusion | flops 94372800 | bytes 2588928 | tf_op jit(solution)/shard_map/rke,heqw->rqhkw/dot_general | solution.py:132
  109.5 9.3 %copy.59 = f32[8,32,32,8,8]{1,2,4,0,3:T(8,128)} copy(f32[8,32,32,8,8]{2,4,3,1,0:T(8,128)} %fusion.12) | data formatting | bytes 4194304 | tf_op jit(solution)/shard_map/rke,heqw->rqhkw/dot_general | solution.py:132
  118.8 0.0 all-gather.3.cloned.1.call-done
  118.8 0.0 copy-start.4
  118.9 3.9 %convolution_convert_fusion.2 = bf16[256,1024]{1,0:T(8,128)(2,1)S(1)} fusion(bf16[256,2048]{1,0:T(8,128)(2,1)} %all-gather.3.cloned.1.call-done, bf16[2048,1024]{1,0:T(8,128)(2,1)} %param.23), kind=kOutput, calls=%fused_computation.35 | convolution fusion | flops 1074003968 | bytes 5767168 | tf_op jit(solution)/shard_map/dot_general | solution.py:43
  122.8 0.1 copy-done.10
  122.9 1.3 convolution_convert_fusion.3
  124.2 0.1 fusion.46
  124.3 1.3 collective-permute-start
  125.6 1.3 collective-permute-start.1
  126.9 1.3 fusion.32
  128.2 0.1 copy.82
  128.3 0.1 copy.61
  128.4 16.8 %collective-permute-done = bf16[2,4,32,1024]{3,2,0,1:T(8,128)(2,1)S(1)} collective-permute-done((bf16[2,4,32,1024]{3,2,0,1:T(8,128)(2,1)S(1)}, bf16[2,4,32,1024]{3,2,0,1:T(8,128)(2,1)S(1)}, u32[]{:S(2)}, u32[]{:S(2)}) %collective-permute-start) | collective-permute-done | bytes 524320 | tf_op jit(solution)/shard_map/ppermute | solution.py:23
  145.3 0.0 collective-permute-done.1
  145.3 0.3 pad_maximum_fusion
  145.5 4.9 %gather_fusion = bf16[8,2,8,32,1024]{4,3,1,2,0:T(8,128)(2,1)} fusion(bf16[2,16,32,1024]{3,2,0,1:T(8,128)(2,1)S(1)} %pad_maximum_fusion, s32[8]{0:T(128)S(1)} %shift-left_bitcast_fusion), kind=kCustom, calls=%fused_computation | custom fusion | bytes 16777344 | tf_op jit(solution)/shard_map/vmap()/gather | solution.py:109
  150.4 4.0 %fusion.66 = (bf16[8,1,8,32,1024]{4,3,1,2,0:T(8,128)(2,1)S(1)}, bf16[8,1,8,32,1024]{4,3,1,2,0:T(8,128)(2,1)S(1)}) fusion(bf16[8,2,8,32,1024]{4,3,1,2,0:T(8,128)(2,1)} %gather_fusion), kind=kLoop, calls=%fused_computation.99 | loop fusion | bytes 16777216 | tf_op jit(solution)/shard_map/slice | solution.py:113
  154.4 0.0 slice-start
  154.4 1.1 copy.81
  155.5 0.0 slice-start.1
  155.5 3.3 %copy.80 = bf16[256,8,8,128]{3,2,1,0:T(8,128)(2,1)} copy(bf16[256,8,8,128]{3,1,2,0:T(8,128)(2,1)S(1)} %bitcast.137) | data formatting | bytes 8388608
  158.8 1.3 slice-done.1
  160.1 4.3 %fusion.68 = (f32[8,32,8]{1,2,0:T(8,128)S(1)}, f32[8,32,8,8,32]{1,4,3,2,0:T(8,128)}) fusion(f32[8,32,32,8,8]{1,2,4,0,3:T(8,128)S(1)} %bitcast.133, bf16[8,32,8,128,1]{3,2,1,0,4:T(8,128)(2,1)S(1)} %bitcast_bitcast_fusion, bf16[8,8,32,8,128]{4,3,2,1,0:T(8,128)(2,1)S(1)} %bitcast.136, pred[32,32]{0,1:T(8,128)(4,1)S(1)} %fusion.57), kind=kOutput, calls=%fused_computation.101 | convolution fusion | flops 136312832 | bytes 8922112 | tf_op jit(solution)/shard_map/rqhd,rkwhd->rqhkw/dot_general | solution.py:135
  164.4 19.5 %all-gather.5.cloned.1.call-done = bf16[2,1024,1024]{2,1,0:T(8,128)(2,1)} async-done(((bf16[2,64,1024]{2,1,0:T(8,128)(2,1)}), bf16[2,1024,1024]{2,1,0:T(8,128)(2,1)}) %all-gather.5.cloned.1.call-update) | async-done | bytes 4194320 | tf_op jit(solution)/shard_map/all_gather | solution.py:87
  184.0 3.2 %slice_bitcast_fusion = (bf16[128,8,8,128]{3,1,2,0:T(8,128)(2,1)S(1)}, bf16[128,8,8,128]{3,1,2,0:T(8,128)(2,1)S(1)}) fusion(bf16[2,1024,1024]{2,1,0:T(8,128)(2,1)} %all-gather.5.cloned.1.call-done), kind=kLoop, calls=%fused_computation.18 | loop fusion | bytes 8388608
  187.1 0.6 copy.83
  187.8 1.3 fusion.16
  189.1 0.0 slice-start.2
  189.1 0.7 bitcast_reduce_fusion
  189.8 1.9 fusion.3
  191.7 1.0 slice-done.3
  192.7 2.0 fusion.2
  194.8 0.6 copy.84
  195.4 3.3 %fusion.21 = f32[8,32,8,128]{3,1,2,0:T(8,128)S(1)} fusion(bf16[1024,8,128]{2,1,0:T(8,128)(2,1)S(1)} %bitcast.143, f32[8,32,8]{1,0,2:T(8,128)S(1)} %copy.67, f32[8,32,8]{1,0,2:T(8,128)S(1)} %copy.63, f32[8,1024,256]{1,2,0:S(1)} %fusion.16), kind=kOutput, calls=%fused_computation.31 | convolution fusion | flops 545259520 | bytes 11550720 | tf_op jit(solution)/shard_map/rqhc,chd->rqhd/dot_general | solution.py:155
  198.7 2.3 %fusion.29 = bf16[8,32,8,128]{3,1,2,0:T(8,128)(2,1)S(1)} fusion(f32[8,32,8,128]{3,1,2,0:T(8,128)S(1)} %fusion.21, f32[8,32,8,8,32]{1,4,3,2,0:T(8,128)S(1)} %bitcast.135, f32[8,32,8]{1,2,0:T(8,128)S(1)} %copy_add_fusion, f32[8,32,8]{1,2,0:T(8,128)S(1)} %copy_maximum_fusion, bf16[8,8,32,8,128]{4,3,2,1,0:T(8,128)(2,1)S(1)} %bitcast.142), kind=kOutput, calls=%fused_computation.33 | convolution fusion | flops 136314880 | bytes 7880704 | tf_op jit(solution)/shard_map/rqhkw,rkwhd->rqhd/dot_general | solution.py:152
  201.0 0.2 copy.70
  201.2 0.0 copy-start.2
  201.3 0.0 copy-start.1
  201.3 4.5 %convolution_convert_fusion = bf16[256,2048]{1,0:T(8,128)(2,1)} fusion(bf16[1024,2048]{1,0:T(8,128)(2,1)} %param.24, bf16[32,8,8,128]{3,2,1,0:T(8,128)(2,1)S(1)} %bitcast.149), kind=kOutput, calls=%fused_computation.17 | convolution fusion | flops 1074266112 | bytes 5767168 | tf_op jit(solution)/shard_map/dot_general | solution.py:160
  205.7 0.0 reduce-scatter.2.cloned.1.call-update
  205.8 7.1 %reduce-scatter.2.cloned.1.call-done = bf16[128,2048]{1,0:T(8,128)(2,1)} async-done(((bf16[256,2048]{1,0:T(8,128)(2,1)}), bf16[128,2048]{1,0:T(8,128)(2,1)}) %reduce-scatter.2.cloned.1.call-update) | async-done | bytes 524304 | tf_op jit(solution)/shard_map/reduce_scatter | solution.py:159
  212.9 2.0 fusion.40
  (37 shorter events, 0.2 us)
Async XLA Ops:
  6.5 1.0 copy-start
  6.5 94.0 %copy-start.7 = (f32[2048]{0:T(1024)S(1)}, f32[2048]{0:T(1024)}, u32[]{:S(2)}) copy-start(f32[2048]{0:T(1024)} %param.17) | copy-start | bytes 24580
  6.5 94.0 %copy-start.6 = (bf16[64,2048]{1,0:T(8,128)(2,1)S(1)}, bf16[64,2048]{1,0:T(8,128)(2,1)}, u32[]{:S(2)}) copy-start(bf16[64,2048]{1,0:T(8,128)(2,1)} %param.14) | copy-start | bytes 786436
  6.5 112.3 %all-gather.3.cloned.1.call-start = ((), (), s32[]{:S(2)}) async-start(), calls=%async_computation.1 | async-start | bytes 1572864 | tf_op jit(solution)/shard_map/all_gather | solution.py:86
  95.6 88.4 %all-gather.5.cloned.1.call-start = ((), (), s32[]{:S(2)}) async-start(), calls=%async_computation.2 | async-start | bytes 4456448 | tf_op jit(solution)/shard_map/all_gather | solution.py:87
  95.6 4.9 %copy-start.3 = (bf16[2048,1024]{1,0:T(8,128)(2,1)S(1)}, bf16[2048,1024]{1,0:T(8,128)(2,1)}, u32[]{:S(2)}) copy-start(bf16[2048,1024]{1,0:T(8,128)(2,1)} %param.23) | copy-start | bytes 12582916
  96.9 5.4 %copy-start.8 = (f32[16,15,31]{2,0,1:T(8,128)S(1)}, f32[16,15,31]{2,0,1:T(8,128)}, u32[]{:S(2)}) copy-start(f32[16,15,31]{2,0,1:T(8,128)} %param.25) | copy-start | bytes 89284
  102.2 110.6 %reduce-scatter.2.cloned.1.call-start = ((), (), s32[]{:S(2)}) async-start(), calls=%async_computation.3 | async-start | bytes 1572864 | tf_op jit(solution)/shard_map/reduce_scatter | solution.py:159
  118.8 3.9 %copy-start.4 = (bf16[2048,1024]{1,0:T(8,128)(2,1)S(1)}, bf16[2048,1024]{1,0:T(8,128)(2,1)}, u32[]{:S(2)}) copy-start(bf16[2048,1024]{1,0:T(8,128)(2,1)} %param.22) | copy-start | bytes 12582916
  118.9 4.0 %copy-start.10 = (bf16[256,2048]{1,0:T(8,128)(2,1)S(1)}, bf16[256,2048]{1,0:T(8,128)(2,1)}, u32[]{:S(2)}) copy-start(bf16[256,2048]{1,0:T(8,128)(2,1)} %all-gather.3.cloned.1.call-done) | copy-start | bytes 3145732
  122.9 4.0 %copy-start.9 = (bf16[2048,1024]{1,0:T(8,128)(2,1)S(1)}, bf16[2048,1024]{1,0:T(8,128)(2,1)}, u32[]{:S(2)}) copy-start(bf16[2048,1024]{1,0:T(8,128)(2,1)} %param.21) | copy-start | bytes 12582916
  124.3 21.0 %collective-permute-start = (bf16[2,4,32,1024]{3,2,0,1:T(8,128)(2,1)S(1)}, bf16[2,4,32,1024]{3,2,0,1:T(8,128)(2,1)S(1)}, u32[]{:S(2)}, u32[]{:S(2)}) collective-permute-start(bf16[2,4,32,1024]{3,2,0,1:T(8,128)(2,1)S(1)} %get-tuple-element.9), channel_id=1, source_target_pairs={{0,2},{2,4},{4,6},{6,8},{8,10},{10,12},{12,14},{14,16},{16,18},{18... | collective-permute-start | bytes 1572872 | tf_op jit(solution)/shard_map/ppermute | solution.py:23
  125.6 19.6 %collective-permute-start.1 = (bf16[2,4,32,1024]{3,2,0,1:T(8,128)(2,1)S(1)}, bf16[2,4,32,1024]{3,2,0,1:T(8,128)(2,1)S(1)}, u32[]{:S(2)}, u32[]{:S(2)}) collective-permute-start(bf16[2,4,32,1024]{3,2,0,1:T(8,128)(2,1)S(1)} %get-tuple-element.10), channel_id=1, source_target_pairs={{2,0},{4,2},{6,4},{8,6},{10,8},{12,10},{14,12},{16,14},{18,16},{20... | collective-permute-start | bytes 1572872 | tf_op jit(solution)/shard_map/ppermute | solution.py:25
  154.4 4.4 %slice-start = ((s8[8388608]{0:T(1024)(128)(4,1)}), s8[4194304]{0:T(1024)(128)(4,1)S(1)}, s32[]{:S(2)}) async-start(s8[8388608]{0:T(1024)(128)(4,1)} %bitcast.132), calls=%async_computation.4 | async-start | bytes 8388608
  155.5 4.6 %slice-start.1 = ((s8[8388608]{0:T(1024)(128)(4,1)}), s8[4194304]{0:T(1024)(128)(4,1)S(1)}, s32[]{:S(2)}) async-start(s8[8388608]{0:T(1024)(128)(4,1)} %bitcast.132), calls=%async_computation.5 | async-start | bytes 8388608
  189.1 2.6 %slice-start.2 = ((s8[8388608]{0:T(1024)(128)(4,1)}), s8[4194304]{0:T(1024)(128)(4,1)S(1)}, s32[]{:S(2)}) async-start(s8[8388608]{0:T(1024)(128)(4,1)} %bitcast.134), calls=%async_computation.6 | async-start | bytes 8388608
  189.8 2.9 %slice-start.3 = ((s8[8388608]{0:T(1024)(128)(4,1)}), s8[4194304]{0:T(1024)(128)(4,1)S(1)}, s32[]{:S(2)}) async-start(s8[8388608]{0:T(1024)(128)(4,1)} %bitcast.134), calls=%async_computation.7 | async-start | bytes 8388608
  195.4 3.3 %copy-start.5 = (bf16[256,8,8,128]{3,2,1,0:T(8,128)(2,1)S(1)}, bf16[256,8,8,128]{3,2,1,0:T(8,128)(2,1)}, u32[]{:S(2)}) copy-start(bf16[256,8,8,128]{3,2,1,0:T(8,128)(2,1)} %copy.80) | copy-start | bytes 12582916
  201.2 11.7 %copy-start.2 = (bf16[128,2048]{1,0:T(8,128)(2,1)S(1)}, bf16[128,2048]{1,0:T(8,128)(2,1)}, u32[]{:S(2)}) copy-start(bf16[128,2048]{1,0:T(8,128)(2,1)} %param.13) | copy-start | bytes 1572868
  201.3 13.6 %copy-start.1 = (bf16[128,1024]{1,0:T(8,128)(2,1)S(1)}, bf16[128,1024]{1,0:T(8,128)(2,1)}, u32[]{:S(2)}) copy-start(bf16[128,1024]{1,0:T(8,128)(2,1)} %param.18) | copy-start | bytes 786436
Sparse Core Ops, SparseCore 0:
  95.7 4.9 all-gather.2
  103.4 80.5 all-gather.4
  205.9 6.9 reduce-scatter.1
